TPU v7x, 32 devices: a whole 2x2x4 slice. The times are simulated.
32 devices in a mesh: ep: 16 (over z, y, x), tp: 2 (over core).
Axes of the slice: x: 2, y: 2, z: 4, core: 2. Of those that a mesh axis runs over, the one named last changes fastest.
Arguments:
- tokens: bfloat16 [4096, 4096], P('ep'), may hold values from -6 to 6
- cotangent: bfloat16 [4096, 4096], P('ep'), may hold values from -1.5 to 1.5
- gates: float32 [4096, 2], P('ep'), may hold values from 0.05 to 0.95
- experts: int32 [4096, 2], P('ep'), may hold values from 0 to 15, all different within a row; in each aligned block of 256 rows (0 to 255, 256 to 511, ...) at most 48 rows name the same one
- gate_w: bfloat16 [16, 4096, 768], P('ep', None, 'tp'), may hold values from -0.09375 to 0.09375
- up_w: bfloat16 [16, 4096, 768], P('ep', None, 'tp'), may hold values from -0.09375 to 0.09375
- down_w: bfloat16 [16, 768, 4096], P('ep', 'tp'), may hold values from -0.21875 to 0.21875
Outputs:
- grad_tokens: bfloat16 [4096, 4096], P('ep', 'tp')
- grad_gates: float32 [4096, 2], P('ep')
- grad_gate_w: bfloat16 [16, 4096, 768], P('ep', None, 'tp')
- grad_up_w: bfloat16 [16, 4096, 768], P('ep', None, 'tp')
- grad_down_w: bfloat16 [16, 768, 4096], P('ep', 'tp')
- sq_gate: float32 [16, 4096], P('ep')
- sq_up: float32 [16, 4096], P('ep')
- sq_down: float32 [16, 768], P('ep', 'tp')
Inputs may be any that keep to these rules, and one draw needn't show every extreme that they name: In each aligned block of 256 rows no expert is named by more than 48 rows, a bound that some expert reaches in some blocks; the 2 experts of a row differ.
All inputs are finite; a program needn't handle non-finite values.
Results may differ from a plain program's by a relative error of at most 0.024.
Values may be sent and summed in bfloat16 or wider, within the bound.
A program may use at most 192 MiB of HBM per device.

v0:
```python
import jax
import jax.numpy as jnp
from jax import lax
from jax.sharding import PartitionSpec as P


def body(tokens, cotangent, gates, experts, gate_w, up_w, down_w):
    tok_rows = tokens.shape[0]
    top_count = experts.shape[1]
    width = tokens.shape[1]
    n_ep = lax.axis_size("ep")
    capacity = 3 * tok_rows * top_count // (2 * n_ep)
    n_slots = n_ep * capacity
    flat_ids = experts.reshape(-1)
    onehot = (flat_ids[:, None] == jnp.arange(n_ep, dtype=jnp.int32)[None, :]).astype(jnp.int32)
    earlier = jnp.cumsum(onehot, axis=0) - onehot
    slot_of = jnp.sum(earlier * onehot, axis=1)
    target = flat_ids * capacity + slot_of
    placing = (target[None, :] == jnp.arange(n_slots, dtype=jnp.int32)[:, None]).astype(jnp.float32)
    place_tok = jnp.sum(placing.reshape(n_slots, tok_rows, top_count), axis=2).astype(jnp.bfloat16)
    send_gate = jnp.dot(placing, gates.reshape(-1), precision=lax.Precision.HIGHEST)
    n_cores = lax.axis_size("tp")
    share = width // n_cores
    offset = lax.axis_index("tp") * share
    tok_share = lax.dynamic_slice_in_dim(tokens, offset, share, 1)
    cot_share = lax.dynamic_slice_in_dim(cotangent, offset, share, 1)
    send_x = jnp.dot(place_tok, tok_share, preferred_element_type=jnp.float32).astype(jnp.bfloat16)
    send_dy = jnp.dot(place_tok, cot_share, preferred_element_type=jnp.float32).astype(jnp.bfloat16)
    part_x, part_dy, recv_gate = (
        lax.all_to_all(
            send_x.reshape(n_ep, capacity, share), "ep", split_axis=0, concat_axis=0, tiled=True
        ),
        lax.all_to_all(
            send_dy.reshape(n_ep, capacity, share), "ep", split_axis=0, concat_axis=0, tiled=True
        ),
        lax.all_to_all(
            send_gate.reshape(n_ep, capacity).astype(jnp.bfloat16),
            "ep",
            split_axis=0,
            concat_axis=0,
            tiled=True,
        ).astype(jnp.float32),
    )
    stacked = jnp.stack([part_x, part_dy], axis=0)
    joined = lax.all_gather(stacked, "tp", axis=3, tiled=True)
    recv_x = joined[0]
    recv_dy = joined[1]
    recv_x = recv_x.reshape(n_slots, width)
    recv_dy = recv_dy.reshape(n_slots, width)
    recv_gate = recv_gate.reshape(n_slots)
    w_gate = gate_w[0]
    w_up = up_w[0]
    w_down = down_w[0]
    contract_last = (((1,), (1,)), ((), ()))
    contract_first = (((0,), (0,)), ((), ()))
    pre_gate = jnp.dot(recv_x, w_gate, preferred_element_type=jnp.float32)
    pre_up = jnp.dot(recv_x, w_up, preferred_element_type=jnp.float32)
    sigmoid_gate = jax.nn.sigmoid(pre_gate)
    silu_gate = pre_gate * sigmoid_gate
    hidden = (silu_gate * pre_up).astype(jnp.bfloat16)
    hidden_grad = lax.dot_general(
        recv_dy, w_down, contract_last, preferred_element_type=jnp.float32
    )
    gate_part = jnp.sum(hidden.astype(jnp.float32) * hidden_grad, axis=1)
    scaled = recv_gate[:, None] * hidden_grad
    grad_pre_gate = (
        scaled * pre_up * sigmoid_gate * (1.0 + pre_gate * (1.0 - sigmoid_gate))
    ).astype(jnp.bfloat16)
    grad_pre_up = (scaled * silu_gate).astype(jnp.bfloat16)
    weighted = (recv_gate[:, None] * hidden.astype(jnp.float32)).astype(jnp.bfloat16)
    grad_dw = lax.dot_general(
        weighted, recv_dy, contract_first, preferred_element_type=jnp.float32
    ).astype(jnp.bfloat16)
    grad_gw = lax.dot_general(
        recv_x, grad_pre_gate, contract_first, preferred_element_type=jnp.float32
    ).astype(jnp.bfloat16)
    grad_uw = lax.dot_general(
        recv_x, grad_pre_up, contract_first, preferred_element_type=jnp.float32
    ).astype(jnp.bfloat16)
    partial_value = lax.dot_general(
        grad_pre_gate, w_gate, contract_last, preferred_element_type=jnp.float32
    ) + lax.dot_general(grad_pre_up, w_up, contract_last, preferred_element_type=jnp.float32)
    partial_terms = partial_value.astype(jnp.bfloat16).astype(jnp.float32)
    gate_total = lax.psum(gate_part, "tp")
    back_part, back_gate = (
        lax.all_to_all(
            partial_terms.astype(jnp.bfloat16).reshape(n_ep, capacity, width),
            "ep",
            split_axis=0,
            concat_axis=0,
            tiled=True,
        ),
        lax.all_to_all(
            gate_total.reshape(n_ep, capacity).astype(jnp.bfloat16),
            "ep",
            split_axis=0,
            concat_axis=0,
            tiled=True,
        ).astype(jnp.float32),
    )
    summed = lax.psum_scatter(
        back_part.reshape(n_slots, width).astype(jnp.float32).astype(jnp.bfloat16),
        "tp",
        scatter_dimension=1,
        tiled=True,
    )
    grad_tokens = lax.dot_general(
        place_tok, summed, contract_first, preferred_element_type=jnp.float32
    ).astype(jnp.bfloat16)
    grad_gates = jnp.dot(
        back_gate.reshape(n_slots), placing, precision=lax.Precision.HIGHEST
    ).reshape(tok_rows, top_count)
    gw_f = grad_gw.astype(jnp.float32)
    uw_f = grad_uw.astype(jnp.float32)
    dw_f = grad_dw.astype(jnp.float32)
    sq_gate_part = jnp.sum(gw_f * gw_f, axis=1)
    sq_up_part = jnp.sum(uw_f * uw_f, axis=1)
    sq_gate, sq_up = (
        lax.psum(sq_gate_part.astype(jnp.bfloat16), "tp").astype(jnp.float32),
        lax.psum(sq_up_part.astype(jnp.bfloat16), "tp").astype(jnp.float32),
    )
    full_units = w_gate.shape[1] * lax.axis_size("tp")
    sq_gate = sq_gate / full_units
    sq_up = sq_up / full_units
    sq_down = jnp.sum(dw_f * dw_f, axis=1) / width
    return (
        grad_tokens,
        grad_gates,
        grad_gw[None],
        grad_uw[None],
        grad_dw[None],
        sq_gate[None],
        sq_up[None],
        sq_down[None],
    )


def solution(mesh):
    placed = (
        P("ep", None),
        P("ep", None),
        P("ep", None),
        P("ep", None),
        P("ep", None, "tp"),
        P("ep", None, "tp"),
        P("ep", "tp", None),
    )
    return jax.shard_map(
        body,
        mesh=mesh,
        in_specs=placed,
        out_specs=(
            P("ep", "tp"),
            P("ep", None),
            P("ep", None, "tp"),
            P("ep", None, "tp"),
            P("ep", "tp", None),
            P("ep", None),
            P("ep", None),
            P("ep", "tp"),
        ),
        check_vma=False,
    )
```

profile of v0, /device:TPU:15, one launch (start us, length us, event | category | flops | bytes accessed | tf_op | source)
XLA Modules:
  0.0 430.6 jit_solution(4047482938456547458)
XLA Ops:
  11.2 3.9 convolution_convert_fusion.3
  15.1 6.6 %all-to-all-start.2 = ((bf16[16,48,2048]{2,1,0:T(8,128)(2,1)}), bf16[16,48,2048]{2,1,0:T(8,128)(2,1)}, u32[]{:S(2)}, u32[]{:S(2)}) async-start(bf16[16,48,2048]{2,1,0:T(8,128)(2,1)} %bitcast.73), calls=%async_computation.2 | async-start | bytes 6291456 | tf_op jit(solution)/shard_map/all_to_all | solution.py:33
  21.7 3.9 convolution_convert_fusion.4
  25.6 66.9 %all-to-all-done.2 = bf16[16,48,2048]{2,1,0:T(8,128)(2,1)} async-done(((bf16[16,48,2048]{2,1,0:T(8,128)(2,1)}), bf16[16,48,2048]{2,1,0:T(8,128)(2,1)}, u32[]{:S(2)}, u32[]{:S(2)}) %all-to-all-start.2) | async-done | bytes 3145760 | tf_op jit(solution)/shard_map/all_to_all | solution.py:33
  92.5 73.4 %all_to_all.30 = bf16[16,48,2048]{2,1,0:T(8,128)(2,1)S(1)} all-to-all(bf16[16,48,2048]{2,1,0:T(8,128)(2,1)} %bitcast.74), channel_id=1, replica_groups=mesh['ep'=16,'tp'=2] {'ep'}, dimensions={0} | all-to-all | bytes 6291456 | tf_op jit(solution)/shard_map/all_to_all | solution.py:30
  165.9 5.1 %pad_maximum_fusion = bf16[2,16,48,2048]{3,2,1,0:T(8,128)(2,1)} fusion(bf16[1,16,48,2048]{3,2,1,0:T(8,128)(2,1)} %bitcast.7, bf16[1,16,48,2048]{3,2,1,0:T(8,128)(2,1)S(1)} %bitcast.75), kind=kLoop, calls=%fused_computation.1 | loop fusion | flops 3145728 | bytes 12582912 | tf_op jit(solution)/shard_map/stack | solution.py:44
  174.8 8.9 %all_to_all.31 = bf16[16,1,48]{2,1,0:T(2,128)(2,1)S(1)} all-to-all(bf16[16,1,48]{2,1,0:T(2,128)(2,1)S(1)} %copy.66), channel_id=1, replica_groups=mesh['ep'=16,'tp'=2] {'ep'}, dimensions={0} | all-to-all | bytes 3072 | tf_op jit(solution)/shard_map/all_to_all | solution.py:36
  183.9 13.9 %all-gather.2.cloned.1.call-done = bf16[2,16,48,4096]{3,2,1,0:T(8,128)(2,1)} async-done(((bf16[2,16,48,2048]{3,2,1,0:T(8,128)(2,1)}), bf16[2,16,48,4096]{3,2,1,0:T(8,128)(2,1)}) %all-gather.2.cloned.1.call-update) | async-done | bytes 12582928 | tf_op jit(solution)/shard_map/all_gather | solution.py:45
  197.7 5.7 %fusion.33 = (bf16[1,16,48,4096]{3,2,1,0:T(8,128)(2,1)S(1)}, bf16[1,16,48,4096]{3,2,1,0:T(8,128)(2,1)S(1)}) fusion(bf16[2,16,48,4096]{3,2,1,0:T(8,128)(2,1)} %all-gather.2.cloned.1.call-done), kind=kLoop, calls=%fused_computation.64 | loop fusion | bytes 25165824 | tf_op jit(solution)/shard_map/slice | solution.py:47
  203.4 2.6 fusion.2
  207.7 2.6 fusion.5
  210.5 3.9 fusion.14
  214.4 6.4 %fusion = f32[768,4096]{1,0:T(8,128)} fusion(bf16[768,384]{0,1:T(8,128)(2,1)S(1)} %get-tuple-element.62, bf16[1,4096,384]{2,1,0:T(8,128)(2,1)S(1)} %copy-done), kind=kOutput, calls=%fused_computation.10 | convolution fusion | flops 2415919104 | bytes 16318464 | tf_op jit(solution)/shard_map/dot_general | solution.py:80
  220.8 6.5 %add_convert_fusion = bf16[768,4096]{1,0:T(8,128)(2,1)S(1)} fusion(f32[768,4096]{1,0:T(8,128)} %fusion, bf16[768,384]{0,1:T(8,128)(2,1)S(1)} %get-tuple-element.63, bf16[1,4096,384]{2,1,0:T(8,128)(2,1)S(1)} %copy-done.4), kind=kOutput, calls=%fused_computation | convolution fusion | flops 2422210560 | bytes 22609920 | tf_op jit(solution)/shard_map/dot_general | solution.py:82
  227.3 142.5 %all_to_all.32 = bf16[16,48,4096]{2,1,0:T(8,128)(2,1)} all-to-all(bf16[16,48,4096]{2,1,0:T(8,128)(2,1)S(1)} %bitcast.72), channel_id=1, replica_groups=mesh['ep'=16,'tp'=2] {'ep'}, dimensions={0} | all-to-all | bytes 12582912 | tf_op jit(solution)/shard_map/all_to_all | solution.py:86
  369.9 3.9 psum.21
  374.5 5.5 %all-to-all-start.4 = ((bf16[16,1,48]{2,1,0:T(2,128)(2,1)}), bf16[16,1,48]{2,1,0:T(2,128)(2,1)S(1)}, u32[]{:S(2)}, u32[]{:S(2)}) async-start(bf16[16,1,48]{2,1,0:T(2,128)(2,1)} %convert_element_type.132), calls=%async_computation.5 | async-start | bytes 16384 | tf_op jit(solution)/shard_map/all_to_all | solution.py:93
  379.9 9.1 %multiply_reduce_fusion.2 = (bf16[4096]{0:T(1024)(128)(2,1)}, bf16[4096,384]{0,1:T(8,128)(2,1)}) fusion(bf16[768,384]{0,1:T(8,128)(2,1)S(1)} %copy-done.8, bf16[768,4096]{1,0:T(8,128)(2,1)} %bitcast.80), kind=kOutput, calls=%fused_computation.4 | convolution fusion | flops 2422206464 | bytes 10035200 | tf_op jit(solution)/shard_map/dot_general | solution.py:74
  389.0 6.2 %multiply_reduce_fusion.1 = (bf16[4096]{0:T(1024)(128)(2,1)}, bf16[4096,384]{0,1:T(8,128)(2,1)S(1)}) fusion(bf16[768,384]{0,1:T(8,128)(2,1)S(1)} %copy-done.6, bf16[768,4096]{1,0:T(8,128)(2,1)} %bitcast.81), kind=kOutput, calls=%fused_computation.3 | convolution fusion | flops 2422206464 | bytes 10035200 | tf_op jit(solution)/shard_map/dot_general | solution.py:77
  395.2 5.1 %all-reduce = (bf16[4096]{0:T(1024)(128)(2,1)}, bf16[4096]{0:T(1024)(128)(2,1)}) all-reduce(bf16[4096]{0:T(1024)(128)(2,1)} %get-tuple-element.64, bf16[4096]{0:T(1024)(128)(2,1)} %get-tuple-element.66), channel_id=1, replica_groups=mesh['ep'=16,'tp'=2] {'tp'}, use_global_device_ids=true, to_apply=%region_8.9 | all-reduce | flops 8192 | bytes 32768 | tf_op jit(solution)/shard_map/psum | solution.py:119
  401.6 7.3 %multiply_reduce_fusion = (f32[384]{0:T(512)S(1)}, bf16[384,4096]{1,0:T(8,128)(2,1)}) fusion(bf16[768,4096]{1,0:T(8,128)(2,1)} %bitcast.77, bf16[768,384]{0,1:T(8,128)(2,1)} %get-tuple-element.59, f32[768]{0:T(1024)S(1)} %reshape.148), kind=kOutput, calls=%fused_computation.2 | convolution fusion | flops 2423094784 | bytes 10031616 | tf_op jit(solution)/shard_map/dot_general | solution.py:71
  409.4 2.8 copy.69
  412.2 4.8 %copy.68 = bf16[1,4096,384]{2,1,0:T(8,128)(2,1)} copy(bf16[1,4096,384]{1,2,0:T(8,128)(2,1)} %bitcast.82) | data formatting | bytes 6291456
  419.9 3.9 convolution_convert_fusion.5
  (58 shorter events, 15.3 us)
Async XLA Ops:
  7.2 196.2 %copy-start = (bf16[1,4096,384]{2,1,0:T(8,128)(2,1)S(1)}, bf16[1,4096,384]{2,1,0:T(8,128)(2,1)}, u32[]{:S(2)}) copy-start(bf16[1,4096,384]{2,1,0:T(8,128)(2,1)} %param.11) | copy-start | bytes 9437188
  15.1 77.4 %all-to-all-start.2 = ((bf16[16,48,2048]{2,1,0:T(8,128)(2,1)}), bf16[16,48,2048]{2,1,0:T(8,128)(2,1)}, u32[]{:S(2)}, u32[]{:S(2)}) async-start(bf16[16,48,2048]{2,1,0:T(8,128)(2,1)} %bitcast.73), calls=%async_computation.2 | async-start | bytes 6291456 | tf_op jit(solution)/shard_map/all_to_all | solution.py:33
  21.7 176.0 %all-gather.2.cloned.1.call-start = ((), (), s32[]{:S(2)}) async-start(), calls=%async_computation.6 | async-start | bytes 18874368 | tf_op jit(solution)/shard_map/all_gather | solution.py:45
  171.0 0.7 copy-start.9
  171.0 248.9 %reduce-scatter.2.cloned.1.call-start = ((), (), s32[]{:S(2)}) async-start(), calls=%async_computation.7 | async-start | bytes 9437184 | tf_op jit(solution)/shard_map/reduce_scatter | solution.py:101
  203.4 3.2 copy-start.3
  203.4 6.9 %copy-start.2 = (bf16[1,16,48,4096]{3,2,1,0:T(8,128)(2,1)}, bf16[1,16,48,4096]{3,2,1,0:T(8,128)(2,1)S(1)}, u32[]{:S(2)}) copy-start(bf16[1,16,48,4096]{3,2,1,0:T(8,128)(2,1)S(1)} %get-tuple-element.60) | copy-start | bytes 18874372
  203.4 4.2 copy-start.4
  207.7 2.8 copy-start.10
  214.4 6.4 %copy-start.7 = (bf16[768,384]{0,1:T(8,128)(2,1)}, bf16[768,384]{0,1:T(8,128)(2,1)S(1)}, u32[]{:S(2)}) copy-start(bf16[768,384]{0,1:T(8,128)(2,1)S(1)} %get-tuple-element.62) | copy-start | bytes 1769476
  214.4 6.4 %copy-start.5 = (bf16[768,384]{0,1:T(8,128)(2,1)}, bf16[768,384]{0,1:T(8,128)(2,1)S(1)}, u32[]{:S(2)}) copy-start(bf16[768,384]{0,1:T(8,128)(2,1)S(1)} %get-tuple-element.63) | copy-start | bytes 1769476
  369.8 10.1 %copy-start.8 = (bf16[768,384]{0,1:T(8,128)(2,1)S(1)}, bf16[768,384]{0,1:T(8,128)(2,1)}, u32[]{:S(2)}) copy-start(bf16[768,384]{0,1:T(8,128)(2,1)} %copy-done.7) | copy-start | bytes 1769476
  374.5 42.5 %all-to-all-start.4 = ((bf16[16,1,48]{2,1,0:T(2,128)(2,1)}), bf16[16,1,48]{2,1,0:T(2,128)(2,1)S(1)}, u32[]{:S(2)}, u32[]{:S(2)}) async-start(bf16[16,1,48]{2,1,0:T(2,128)(2,1)} %convert_element_type.132), calls=%async_computation.5 | async-start | bytes 16384 | tf_op jit(solution)/shard_map/all_to_all | solution.py:93
  379.9 9.1 %copy-start.6 = (bf16[768,384]{0,1:T(8,128)(2,1)S(1)}, bf16[768,384]{0,1:T(8,128)(2,1)}, u32[]{:S(2)}) copy-start(bf16[768,384]{0,1:T(8,128)(2,1)} %copy-done.5) | copy-start | bytes 1769476
  412.2 11.6 %copy-start.1 = (bf16[1,4096,384]{2,1,0:T(8,128)(2,1)S(1)}, bf16[1,4096,384]{2,1,0:T(8,128)(2,1)}, u32[]{:S(2)}) copy-start(bf16[1,4096,384]{2,1,0:T(8,128)(2,1)} %param.11) | copy-start | bytes 9437188
Sparse Core Ops, SparseCore 0:
  171.1 26.5 all-gather.1
  370.0 15.4 reduce-scatter.1
where the time goes:
time: 432 us; the launch traced here: 431 us
  blocking collectives  234 us (54%)
  waiting for transfers between devices  80.8 us (19%)
  matrix products  58.7 us (14%)
  local copies, waits for them, and re-layouts  22.2 us (5%)
  between operations  14.2 us (3%)
  starting transfers between devices  12.1 us (3%)
  other arithmetic  8.81 us (2%)
    all_to_all x1, blocking collectives, body(): lax.all_to_all(partial_terms.astype(jnp.bfloat16).reshape(n_ep, capacity,...  143 us
    all_to_all x1, blocking collectives, body(): lax.all_to_all(send_x.reshape(n_ep, capacity, share), 'ep', split_axis=0,...  73.4 us
    all_to_all x1, waiting for transfers between devices, body(): lax.all_to_all(send_dy.reshape(n_ep, capacity, share), 'ep', split_axis=0...  66.9 us
    all_gather x1, waiting for transfers between devices, body(): joined = lax.all_gather(stacked, 'tp', axis=3, tiled=True)  13.9 us
    unnamed x26, local copies, waits for them, and re-layouts  11.7 us
    dot_general x1, matrix products, body(): lax.dot_general(recv_x, grad_pre_gate, contract_first, preferred_element_...  9.05 us
    all_to_all x1, blocking collectives, body(): lax.all_to_all(send_gate.reshape(n_ep, capacity).astype(jnp.bfloat16), 'e...  8.92 us
  transfers between devices with their start and end apart: 4, of which 2 were waited for; matrix products, arithmetic and copies ran while one was open for 10% of the time, Pallas kernels for 0%

commit v1 on v0

v1 whole, which is shorter than its diff:
```python
import functools

import jax
import jax.numpy as jnp
from jax import lax
from jax.experimental import pallas as pl
from jax.experimental.pallas import tpu as pltpu
from jax.sharding import PartitionSpec as P

MESH = pl.DeviceIdType.MESH
BF16 = jnp.bfloat16
F32 = jnp.float32
NN = (((1,), (0,)), ((), ()))
NT = (((1,), (1,)), ((), ()))
TN = (((0,), (0,)), ((), ()))


def dot(a, b, dims, precision=None):
    return lax.dot_general(a, b, dims, precision=precision, preferred_element_type=F32)


def kernel(
    n, cap, units, share, groups, tile,
    sx, sdy, sg, wg_in, wu_in, wd_in,
    back, gback, ggw, guw, gdw, sq_out, sqd_out,
    xr, dyr, gr, wg, wu, wd, pg, pu, prod, gpgu, wt, keep, give, got, rg,
    gp, gpp, gt, gcol, sqs, sqr, acc,
    w_sem, s_sem, r_sem, gs_sem, gr_sem, fs_sem, fr_sem,
    ps_sem, pr_sem, qs_sem, qr_sem, bs_sem, br_sem, hs_sem, hr_sem, o_sem, e_sem,
):
    me = lax.axis_index("ep")
    t = lax.axis_index("tp")
    other = lax.axis_size("tp") - 1 - t
    per = n // groups
    rows_g = per * cap

    def rows(s):
        return pl.ds(pl.multiple_of(s * cap, 16), cap)

    def remote(src, dst, send, recv, **where):
        return pltpu.make_async_remote_copy(
            src_ref=src, dst_ref=dst, send_sem=send, recv_sem=recv,
            device_id=where, device_id_type=MESH,
        )

    def loop(count, fn):
        def step(i, carry):
            fn(i)
            return carry
        lax.fori_loop(0, count, step, 0)

    def peer(k):
        return lax.rem(me + n // 2 + k + jnp.where(k >= n - n // 2, 1, 0), n)

    barrier = pltpu.get_barrier_semaphore()
    loop(n - 1, lambda k: pl.semaphore_signal(
        barrier, inc=1, device_id={"ep": peer(k)}, device_id_type=MESH))
    pl.semaphore_signal(barrier, inc=1, device_id={"tp": other}, device_id_type=MESH)
    pl.semaphore_wait(barrier, n)

    ins = ((sx, xr), (sdy, dyr))
    for which, (src, dst) in enumerate(ins):
        def send(k, which=which, src=src, dst=dst):
            d = peer(k)
            remote(src.at[d], dst.at[t, rows(me)], s_sem.at[which, d],
                   r_sem.at[which, me], ep=d).start()
        loop(n - 1, send)
        pltpu.make_async_copy(src.at[me], dst.at[t, rows(me)], r_sem.at[which, me]).start()
        if which == 0:
            def send_gate(k):
                d = peer(k)
                remote(sg.at[d], gr.at[me], gs_sem.at[d], gr_sem.at[me], ep=d).start()
            loop(n - 1, send_gate)
            pltpu.make_async_copy(sg.at[me], gr.at[me], gr_sem.at[me]).start()
            loads = [
                pltpu.make_async_copy(a, b, w_sem.at[i])
                for i, (a, b) in enumerate(((wg_in, wg), (wu_in, wu), (wd_in, wd)))
            ]
            for load in loads:
                load.start()

    def order(i):
        return lax.rem(me // per + groups // 2 + i, groups)

    def arrive(which, g):
        src, dst = ins[which]

        def pass_on(j):
            s = g * per + j
            pltpu.make_async_copy(src.at[0], dst.at[t, rows(s)], r_sem.at[which, s]).wait()
            remote(dst.at[t, rows(s)], dst.at[t, rows(s)], fs_sem.at[which, s],
                   fr_sem.at[which, s], tp=other).start()

        def joined(j):
            s = g * per + j
            remote(dst.at[other, rows(s)], dst.at[other, rows(s)], fs_sem.at[which, s],
                   fr_sem.at[which, s], tp=other).wait_recv()

        loop(per, pass_on)
        loop(per, joined)

    def span(g):
        return pl.ds(pl.multiple_of(g * rows_g, 16), rows_g)

    for load in loads:
        load.wait()

    def forward(i):
        g = order(i)
        arrive(0, g)
        r = span(g)
        pg[r, :] = dot(xr[0, r, :], wg[0], NN) + dot(xr[1, r, :], wg[1], NN)
        pu[r, :] = dot(xr[0, r, :], wu[0], NN) + dot(xr[1, r, :], wu[1], NN)

    loop(groups, forward)

    def exchange(g):
        r = span(g)
        grp = pl.ds(g * per, per)
        return (
            remote(give.at[r], got.at[r], ps_sem.at[g], pr_sem.at[g], tp=other),
            remote(gp.at[grp], gpp.at[grp], qs_sem.at[g], qr_sem.at[g], tp=other),
        )

    def back_copies(s):
        return (
            remote(rg.at[rows(s)], back.at[me], bs_sem.at[s], br_sem.at[me], ep=s),
            remote(gt.at[s], gback.at[me], hs_sem.at[s], hr_sem.at[me], ep=s),
        )

    def finish(g):
        for copy in exchange(g):
            copy.wait_recv()

        def one(j):
            s = g * per + j
            r = rows(s)
            rg[r, :] = (keep[r, :].astype(F32) + got[r, :].astype(F32)).astype(BF16)
            gt[s] = gp[s] + gpp[s]

        loop(per, one)

        def out(j):
            s = g * per + j

            @pl.when(s == me)
            def _():
                pltpu.make_async_copy(rg.at[rows(s)], back.at[me], br_sem.at[me]).start()
                pltpu.make_async_copy(gt.at[s], gback.at[me], hr_sem.at[me]).start()

            @pl.when(s != me)
            def _():
                for copy in back_copies(s):
                    copy.start()

        loop(per, out)

    ones_units = jnp.ones((8, units), F32)

    def backward(i):
        g = order(i)
        arrive(1, g)

        def gates_in(j):
            s = g * per + j
            pltpu.make_async_copy(sg.at[0], gr.at[s], gr_sem.at[s]).wait()
            column = jnp.transpose(gr[s])
            gcol[rows(s), :] = jnp.broadcast_to(column[:cap, 0:1], (cap, 128))

        loop(per, gates_in)
        r = span(g)
        dh = dot(dyr[0, r, :], wd[:, :share], NT) + dot(dyr[1, r, :], wd[:, share:], NT)
        a = pg[r, :]
        b = pu[r, :]
        gate = gcol[r, 0:1]
        sig = jax.nn.sigmoid(a)
        silu = a * sig
        hidden = (silu * b).astype(BF16).astype(F32)
        prod[...] = hidden * dh
        scaled = gate * dh
        gpg = (scaled * b * sig * (1.0 + a * (1.0 - sig))).astype(BF16)
        gpu = (scaled * silu).astype(BF16)
        gpgu[r, :units] = gpg
        gpgu[r, units:] = gpu
        wt[r, :] = (gate * hidden).astype(BF16)

        def part(c):
            cols = pl.ds(pl.multiple_of(c * tile, tile), tile)
            for half, dst in ((other, give), (t, keep)):
                dst[r, cols] = (
                    dot(gpgu[r, :units], wg[half, cols, :], NT)
                    + dot(gpgu[r, units:], wu[half, cols, :], NT)
                ).astype(BF16)

        loop(share // tile, part)

        def gate_sum(j):
            p = prod[pl.ds(pl.multiple_of(j * cap, 16), cap), :]
            gp[g * per + j, :, :cap] = dot(ones_units, p, NT, lax.Precision.HIGHEST)

        loop(per, gate_sum)
        for copy in exchange(g):
            copy.start()

        @pl.when(i > 0)
        def _():
            finish(order(i - 1 + groups))

    gp[...] = jnp.zeros_like(gp)
    loop(groups, backward)
    finish(order(groups - 1))

    acc[...] = jnp.zeros_like(acc)
    for h in range(2):
        def grads(c, h=h):
            cols = pl.ds(pl.multiple_of(c * tile, tile), tile)
            q = dot(xr[h, :, cols], gpgu[...], TN).astype(BF16)
            wg[h, cols, :] = q[:, :units]
            wu[h, cols, :] = q[:, units:]
            f = q.astype(F32)
            f = f * f
            sqs[0, h, c] = dot(ones_units, f[:, :units], NT, lax.Precision.HIGHEST)
            sqs[1, h, c] = dot(ones_units, f[:, units:], NT, lax.Precision.HIGHEST)
            d = dot(wt[...], dyr[h, :, cols], TN).astype(BF16)
            wd[:, pl.ds(pl.multiple_of(h * share + c * tile, tile), tile)] = d
            d = d.astype(F32)
            acc[...] += d * d

        loop(share // tile, grads)

    stores = [
        pltpu.make_async_copy(a, b, o_sem.at[i])
        for i, (a, b) in enumerate(((wg, ggw), (wu, guw), (wd, gdw)))
    ]
    for store in stores:
        store.start()
    squares = remote(sqs, sqr, e_sem.at[0], e_sem.at[1], tp=other)
    squares.start()
    sqd_out[...] = dot(jnp.ones((8, tile), F32), acc[...], NT, lax.Precision.HIGHEST)
    squares.wait()
    sq_out[...] = sqs[...] + sqr[...]
    for store in stores:
        store.wait()

    def drain(k):
        d = peer(k)
        for which, (src, dst) in enumerate(ins):
            remote(src.at[d], dst.at[t, rows(me)], s_sem.at[which, d],
                   r_sem.at[which, me], ep=d).wait_send()
        remote(sg.at[d], gr.at[me], gs_sem.at[d], gr_sem.at[me], ep=d).wait_send()
        for copy in back_copies(d):
            copy.wait_send()

    loop(n - 1, drain)

    def drain_pair(s):
        for which, (src, dst) in enumerate(ins):
            remote(dst.at[t, rows(s)], dst.at[t, rows(s)], fs_sem.at[which, s],
                   fr_sem.at[which, s], tp=other).wait_send()
        pltpu.make_async_copy(rg.at[rows(s)], back.at[s], br_sem.at[s]).wait()
        pltpu.make_async_copy(gt.at[s], gback.at[s], hr_sem.at[s]).wait()

    loop(n, drain_pair)

    def drain_group(g):
        for copy in exchange(g):
            copy.wait_send()

    loop(groups, drain_group)


def fused(n, cap, send_x, send_dy, send_gate, w_gate, w_up, w_down):
    width, units = w_gate.shape
    share = send_x.shape[2]
    total = n * cap
    groups = 4
    tile = 512
    any_spec = pl.BlockSpec(memory_space=pl.ANY)
    vmem = pl.BlockSpec(memory_space=pltpu.VMEM)
    sq_shape = (2, 2, share // tile, 8, tile)
    dma = pltpu.SemaphoreType.DMA
    shape = jax.ShapeDtypeStruct
    return pl.pallas_call(
        functools.partial(kernel, n, cap, units, share, groups, tile),
        out_shape=(
            shape((n, cap, share), BF16),
            shape((n, 8, 128), F32),
            shape((2, share, units), BF16),
            shape((2, share, units), BF16),
            shape((units, width), BF16),
            shape(sq_shape, F32),
            shape((8, units), F32),
        ),
        in_specs=[any_spec] * 6,
        out_specs=(any_spec,) * 5 + (vmem, vmem),
        scratch_shapes=[
            pltpu.VMEM((2, total, share), BF16),
            pltpu.VMEM((2, total, share), BF16),
            pltpu.VMEM((n, 8, 128), F32),
            pltpu.VMEM((2, share, units), BF16),
            pltpu.VMEM((2, share, units), BF16),
            pltpu.VMEM((units, width), BF16),
            pltpu.VMEM((total, units), F32),
            pltpu.VMEM((total, units), F32),
            pltpu.VMEM((total // groups, units), F32),
            pltpu.VMEM((total, 2 * units), BF16),
            pltpu.VMEM((total, units), BF16),
            pltpu.VMEM((total, share), BF16),
            pltpu.VMEM((total, share), BF16),
            pltpu.VMEM((total, share), BF16),
            pltpu.VMEM((total, share), BF16),
            pltpu.VMEM((n, 8, 128), F32),
            pltpu.VMEM((n, 8, 128), F32),
            pltpu.VMEM((n, 8, 128), F32),
            pltpu.VMEM((total, 128), F32),
            pltpu.VMEM(sq_shape, F32),
            pltpu.VMEM(sq_shape, F32),
            pltpu.VMEM((units, tile), F32),
            dma((3,)), dma((2, n)), dma((2, n)), dma((n,)), dma((n,)), dma((2, n)), dma((2, n)),
            dma((groups,)), dma((groups,)), dma((groups,)), dma((groups,)),
            dma((n,)), dma((n,)), dma((n,)), dma((n,)), dma((3,)), dma((2,)),
        ],
        compiler_params=pltpu.CompilerParams(
            collective_id=0, has_side_effects=True, vmem_limit_bytes=63 << 20
        ),
    )(send_x, send_dy, send_gate,
      w_gate.reshape(2, share, units), w_up.reshape(2, share, units), w_down)


def body(tokens, cotangent, gates, experts, gate_w, up_w, down_w):
    tok_rows, width = tokens.shape
    top_count = experts.shape[1]
    n_ep = lax.axis_size("ep")
    n_cores = lax.axis_size("tp")
    capacity = 3 * tok_rows * top_count // (2 * n_ep)
    cap = -(-capacity // 16) * 16
    n_slots = n_ep * cap
    flat_ids = experts.reshape(-1)
    onehot = (flat_ids[:, None] == jnp.arange(n_ep, dtype=jnp.int32)[None, :]).astype(jnp.int32)
    earlier = jnp.cumsum(onehot, axis=0) - onehot
    slot_of = jnp.sum(earlier * onehot, axis=1)
    target = flat_ids * cap + slot_of
    placing = (target[None, :] == jnp.arange(n_slots, dtype=jnp.int32)[:, None]).astype(F32)
    place_tok = jnp.sum(placing.reshape(n_slots, tok_rows, top_count), axis=2).astype(BF16)
    send_gate = jnp.dot(placing, gates.reshape(-1), precision=lax.Precision.HIGHEST)
    send_gate = jnp.pad(send_gate.reshape(n_ep, 1, cap), ((0, 0), (0, 7), (0, 128 - cap)))
    share = width // n_cores
    offset = lax.axis_index("tp") * share
    tok_share = lax.dynamic_slice_in_dim(tokens, offset, share, 1)
    cot_share = lax.dynamic_slice_in_dim(cotangent, offset, share, 1)
    send_x = jnp.dot(place_tok, tok_share, preferred_element_type=F32).astype(BF16)
    send_dy = jnp.dot(place_tok, cot_share, preferred_element_type=F32).astype(BF16)
    back, gback, ggw, guw, gdw, sq, sqd = fused(
        n_ep, cap, send_x.reshape(n_ep, cap, share), send_dy.reshape(n_ep, cap, share),
        send_gate, gate_w[0], up_w[0], down_w[0],
    )
    grad_tokens = lax.dot_general(
        place_tok, back.reshape(n_slots, share), TN, preferred_element_type=F32
    ).astype(BF16)
    grad_gates = jnp.dot(
        gback[:, 0, :cap].reshape(n_slots), placing, precision=lax.Precision.HIGHEST
    ).reshape(tok_rows, top_count)
    full_units = gate_w.shape[2] * n_cores
    sq = sq[:, :, :, 0, :].reshape(2, width) / full_units
    return (
        grad_tokens,
        grad_gates,
        ggw.reshape(gate_w.shape),
        guw.reshape(up_w.shape),
        gdw[None],
        sq[0][None],
        sq[1][None],
        sqd[0:1] / width,
    )


def solution(mesh):
    placed = (
        P("ep", None),
        P("ep", None),
        P("ep", None),
        P("ep", None),
        P("ep", None, "tp"),
        P("ep", None, "tp"),
        P("ep", "tp", None),
    )
    return jax.shard_map(
        body,
        mesh=mesh,
        in_specs=placed,
        out_specs=(
            P("ep", "tp"),
            P("ep", None),
            P("ep", None, "tp"),
            P("ep", None, "tp"),
            P("ep", "tp", None),
            P("ep", None),
            P("ep", None),
            P("ep", "tp"),
        ),
        check_vma=False,
    )
```

time: 432 us -> 257 us (0.59)
  blocking collectives: 234 us -> 0 us
  Pallas kernels: 0 us -> 225 us
  waiting for transfers between devices: 80.8 us -> 0 us
  matrix products: 58.7 us -> 12.5 us
  between operations: 14.2 us -> 0.73 us
  starting transfers between devices: 12.1 us -> 0 us
  local copies, waits for them, and re-layouts: 22.2 us -> 14.1 us
    pallas_call x0 -> x1, Pallas kernels: none -> 225 us  [fused(): pl.pallas_call(functools.partial(kernel, n, cap, units, share, groups, ti...]
    all_to_all x3 -> x0, blocking collectives: 225 us -> none  [the longest x1 143 us: body(): lax.all_to_all(partial_terms.astype(jnp.bfloat16).reshape(n_ep, capacity,...]
    all_to_all x2 -> x0, waiting for transfers between devices: 66.9 us -> none  [the longest x1 66.9 us: body(): lax.all_to_all(send_dy.reshape(n_ep, capacity, share), 'ep', split_axis=0...]
    dot_general x12 -> x4, matrix products: 57.4 us -> 11.3 us  [the longest x1 3.89 us: body(): jnp.dot(place_tok, cot_share, preferred_element_type=F32).astype(BF16)]
    all_gather x1 -> x0, waiting for transfers between devices: 13.9 us -> none  [body(): joined = lax.all_gather(stacked, 'tp', axis=3, tiled=True)]
    all_to_all x2 -> x0, starting transfers between devices: 12 us -> none  [the longest x1 6.58 us: body(): lax.all_to_all(send_dy.reshape(n_ep, capacity, share), 'ep', split_axis=0...]
    psum x2 -> x0, blocking collectives: 8.97 us -> none  [the longest x1 5.06 us: body(): lax.psum(sq_gate_part.astype(jnp.bfloat16), 'tp').astype(jnp.float32)]
    another operation x3 -> x2, other arithmetic: 6.26 us -> 1.19 us  [the longest x1 5.07 us: body(): stacked = jnp.stack([part_x, part_dy], axis=0)]
  transfers between devices with their start and end apart: 4 -> 0, of which waited for: 2 -> 0; matrix products, arithmetic and copies ran while one was open for 10% -> 0% of each run, Pallas kernels for 0% -> 0%
where the time goes in v1:
time: 257 us
  Pallas kernels  225 us (88%)
  local copies, waits for them, and re-layouts  14.1 us (5%)
  matrix products  12.5 us (5%)
  other arithmetic  4.58 us (2%)
    pallas_call x1, Pallas kernels, fused(): pl.pallas_call(functools.partial(kernel, n, cap, units, share, groups, ti...  225 us
    unnamed x11, local copies, waits for them, and re-layouts  10.3 us

profile of v1, /device:TPU:15, one launch (start us, length us, event | category | flops | bytes accessed | tf_op | source)
XLA Modules:
  0.0 257.0 jit_solution(17131096638502251257)
XLA Ops:
  0.6 0.8 copy.32
  1.5 0.1 eq.75
  1.8 1.2 reduce-window.6
  2.9 0.2 slice_reduce_fusion
  3.5 0.7 multiply_add_fusion.2
  4.2 0.8 copy.36
  5.0 0.1 reshape.122
  5.2 1.3 fusion.5
  6.5 0.7 pad.4.sg
  7.1 0.3 convert_reduce_fusion
  7.5 3.9 %convolution_convert_fusion = bf16[768,2048]{1,0:T(8,128)(2,1)} fusion(bf16[256,4096]{1,0:T(8,128)(2,1)} %param.8, s32[]{:T(128)S(6)} %select_n.4, bf16[768,256]{1,0:T(8,128)(2,1)S(1)} %convert_reduce_fusion), kind=kOutput, calls=%fused_computation | convolution fusion | flops 806879232 | bytes 4587524 | tf_op jit(solution)/shard_map/dot_general | solution.py:352
  11.3 2.7 %convolution_convert_fusion.1 = bf16[768,2048]{1,0:T(8,128)(2,1)} fusion(bf16[256,4096]{1,0:T(8,128)(2,1)S(1)} %copy-done.2, s32[]{:T(128)S(6)} %select_n.4, bf16[768,256]{1,0:T(8,128)(2,1)S(1)} %convert_reduce_fusion), kind=kOutput, calls=%fused_computation.1 | convolution fusion | flops 806879232 | bytes 4587524 | tf_op jit(solution)/shard_map/dot_general | solution.py:351
  14.0 225.1 %shard_map.134 = (bf16[16,48,2048]{2,1,0:T(8,128)(2,1)}, f32[16,8,128]{2,1,0:T(8,128)}, bf16[2,2048,384]{2,1,0:T(8,128)(2,1)}, bf16[2,2048,384]{2,1,0:T(8,128)(2...) custom-call(bf16[16,48,2048]{2,1,0:T(8,128)(2,1)} %bitcast.45, ...), custom_call_target="tpu_custom_call" | custom-call | tf_op jit(solution)/shard_map/pallas_call | solution.py:283
  239.1 3.9 %convolution_convert_fusion.2 = bf16[256,2048]{1,0:T(8,128)(2,1)} fusion(bf16[768,2048]{1,0:T(8,128)(2,1)} %bitcast.55, bf16[768,256]{1,0:T(8,128)(2,1)S(1)} %convert_reduce_fusion), kind=kOutput, calls=%fused_computation.2 | convolution fusion | flops 805830656 | bytes 4587520 | tf_op jit(solution)/shard_map/dot_general | solution.py:357
  242.9 1.3 slice_multiply_fusion.1
  244.2 0.9 slice_reduce_fusion.1
  245.2 1.0 slice_multiply_fusion
  246.1 0.6 fusion.22
  246.8 0.8 fusion.1
  247.6 0.7 copy.38
  248.3 4.0 %copy.44 = bf16[1,4096,384]{2,1,0:T(8,128)(2,1)} copy(bf16[1,4096,384]{2,1,0:T(8,128)(2,1)} %bitcast.48) | data formatting | bytes 6291456
  252.3 1.7 copy.45
  254.0 1.4 copy-done
  255.3 1.7 copy.46
  (15 shorter events, 0.6 us)
Async XLA Ops:
  6.5 4.9 %copy-start.2 = (bf16[256,4096]{1,0:T(8,128)(2,1)S(1)}, bf16[256,4096]{1,0:T(8,128)(2,1)}, u32[]{:S(2)}) copy-start(bf16[256,4096]{1,0:T(8,128)(2,1)} %param.7) | copy-start | bytes 6291460
  248.3 4.0 %copy-start.1 = (bf16[2,2048,384]{2,1,0:T(8,128)(2,1)S(1)}, bf16[2,2048,384]{2,1,0:T(8,128)(2,1)}, u32[]{:S(2)}) copy-start(bf16[2,2048,384]{2,1,0:T(8,128)(2,1)} %get-tuple-element.18) | copy-start | bytes 9437188
  252.3 3.0 %copy-start = (bf16[384,4096]{1,0:T(8,128)(2,1)S(1)}, bf16[384,4096]{1,0:T(8,128)(2,1)}, u32[]{:S(2)}) copy-start(bf16[384,4096]{1,0:T(8,128)(2,1)} %get-tuple-element.19) | copy-start | bytes 9437188

commit v2 on v1

--- a/solution.py
+++ b/solution.py
@@ -238,7 +238,12 @@
     squares.start()
     sqd_out[...] = dot(jnp.ones((8, tile), F32), acc[...], NT, lax.Precision.HIGHEST)
     squares.wait()
-    sq_out[...] = sqs[...] + sqr[...]
+    for which in range(2):
+        for h in range(2):
+            for c in range(share // tile):
+                start = h * share + c * tile
+                both = sqs[which, h, c] + sqr[which, h, c]
+                sq_out[which : which + 1, start : start + tile] = both[0:1, :]
     for store in stores:
         store.wait()
 
@@ -273,7 +278,7 @@
     width, units = w_gate.shape
     share = send_x.shape[2]
     total = n * cap
-    groups = 4
+    groups = 8
     tile = 512
     any_spec = pl.BlockSpec(memory_space=pl.ANY)
     vmem = pl.BlockSpec(memory_space=pltpu.VMEM)
@@ -288,7 +293,7 @@
             shape((2, share, units), BF16),
             shape((2, share, units), BF16),
             shape((units, width), BF16),
-            shape(sq_shape, F32),
+            shape((2, width), F32),
             shape((8, units), F32),
         ),
         in_specs=[any_spec] * 6,
@@ -361,7 +366,7 @@
         gback[:, 0, :cap].reshape(n_slots), placing, precision=lax.Precision.HIGHEST
     ).reshape(tok_rows, top_count)
     full_units = gate_w.shape[2] * n_cores
-    sq = sq[:, :, :, 0, :].reshape(2, width) / full_units
+    sq = sq / full_units
     return (
         grad_tokens,
         grad_gates,

time: 257 us -> 278 us (1.082)
  the two profiles are of different devices: /device:TPU:15 before, /device:TPU:29 now
where the time goes in v2:
time: 278 us
  Pallas kernels  247 us (89%)
  local copies, waits for them, and re-layouts  14.1 us (5%)
  matrix products  12.5 us (4%)
  other arithmetic  3.62 us (1%)
    pallas_call x1, Pallas kernels, fused(): pl.pallas_call(functools.partial(kernel, n, cap, units, share, groups, ti...  247 us
    unnamed x13, local copies, waits for them, and re-layouts  10.3 us

profile of v2, /device:TPU:29, one launch (start us, length us, event | category | flops | bytes accessed | tf_op | source)
XLA Modules:
  0.0 277.9 jit_solution(10718307557133285700)
XLA Ops:
  0.6 0.8 copy.32
  1.5 0.1 eq.75
  1.6 0.1 eq.79
  1.8 1.2 reduce-window.6
  2.9 0.2 slice_reduce_fusion
  3.5 0.7 multiply_add_fusion.2
  4.2 0.8 copy.36
  5.0 0.1 reshape.118
  5.2 1.3 fusion.5
  6.5 0.7 pad.4.sg
  7.1 0.3 convert_reduce_fusion
  7.5 3.9 %convolution_convert_fusion = bf16[768,2048]{1,0:T(8,128)(2,1)} fusion(bf16[256,4096]{1,0:T(8,128)(2,1)} %param.8, s32[]{:T(128)S(6)} %select_n.4, bf16[768,256]{1,0:T(8,128)(2,1)S(1)} %convert_reduce_fusion), kind=kOutput, calls=%fused_computation | convolution fusion | flops 806879232 | bytes 4587524 | tf_op jit(solution)/shard_map/dot_general | solution.py:357
  11.4 2.7 convolution_convert_fusion.1
  14.0 246.8 %shard_map.134 = (bf16[16,48,2048]{2,1,0:T(8,128)(2,1)}, f32[16,8,128]{2,1,0:T(8,128)}, bf16[2,2048,384]{2,1,0:T(8,128)(2,1)}, bf16[2,2048,384]{2,1,0:T(8,128)(2...) custom-call(bf16[16,48,2048]{2,1,0:T(8,128)(2,1)} %bitcast.43, ...), custom_call_target="tpu_custom_call" | custom-call | tf_op jit(solution)/shard_map/pallas_call | solution.py:288
  260.9 3.9 %convolution_convert_fusion.2 = bf16[256,2048]{1,0:T(8,128)(2,1)} fusion(bf16[768,2048]{1,0:T(8,128)(2,1)} %bitcast.51, bf16[768,256]{1,0:T(8,128)(2,1)S(1)} %convert_reduce_fusion), kind=kOutput, calls=%fused_computation.2 | convolution fusion | flops 805830656 | bytes 4587520 | tf_op jit(solution)/shard_map/dot_general | solution.py:362
  264.7 1.3 slice_multiply_fusion
  266.0 0.9 slice_reduce_fusion.1
  267.0 0.6 fusion.22
  267.6 0.8 fusion.1
  268.5 0.7 copy.38
  269.2 4.0 %copy.44 = bf16[1,4096,384]{2,1,0:T(8,128)(2,1)} copy(bf16[1,4096,384]{2,1,0:T(8,128)(2,1)} %bitcast.46) | data formatting | bytes 6291456
  273.2 1.7 copy.45
  274.9 1.4 copy-done
  276.2 1.7 copy.46
  (17 shorter events, 0.5 us)
Async XLA Ops:
  6.5 4.9 %copy-start.2 = (bf16[256,4096]{1,0:T(8,128)(2,1)S(1)}, bf16[256,4096]{1,0:T(8,128)(2,1)}, u32[]{:S(2)}) copy-start(bf16[256,4096]{1,0:T(8,128)(2,1)} %param.7) | copy-start | bytes 6291460
  260.8 6.1 %copy-start.3 = (f32[2,4096]{1,0:T(2,128)S(1)}, f32[2,4096]{1,0:T(2,128)}, u32[]{:S(2)}) copy-start(f32[2,4096]{1,0:T(2,128)} %get-tuple-element.20) | copy-start | bytes 98308
  269.2 4.0 %copy-start.1 = (bf16[2,2048,384]{2,1,0:T(8,128)(2,1)S(1)}, bf16[2,2048,384]{2,1,0:T(8,128)(2,1)}, u32[]{:S(2)}) copy-start(bf16[2,2048,384]{2,1,0:T(8,128)(2,1)} %get-tuple-element.18) | copy-start | bytes 9437188
  273.2 3.0 %copy-start = (bf16[384,4096]{1,0:T(8,128)(2,1)S(1)}, bf16[384,4096]{1,0:T(8,128)(2,1)}, u32[]{:S(2)}) copy-start(bf16[384,4096]{1,0:T(8,128)(2,1)} %get-tuple-element.19) | copy-start | bytes 9437188
